TPU v7x, 32 devices: a whole 2x2x4 slice. The times are simulated.
32 devices in a mesh: dp: 2 (over x), kv: 8 (over z, y), tp: 2 (over core).
Axes of the slice: x: 2, y: 2, z: 4, core: 2. Of those that a mesh axis runs over, the one named last changes fastest.
Arguments:
- tokens: bfloat16 [16, 2048], P('dp', 'kv'), may hold values from -6 to 6
- lengths: int32 [16], P('dp'), may hold values from 1 to 2047, as said below
- query_weight: bfloat16 [2048, 2048], P('kv', 'tp'), may hold values from -0.125 to 0.125
- key_weight: bfloat16 [2048, 256], P('kv', 'tp'), may hold values from -0.125 to 0.125
- value_weight: bfloat16 [2048, 256], P('kv', 'tp'), may hold values from -0.125 to 0.125
- query_gain: float32 [64], replicated, may hold values from 0.1 to 1.9
- key_gain: float32 [64], replicated, may hold values from 0.1 to 1.9
- lambdas: float32 [16], P('tp'), may hold values from 0.3 to 0.8
- head_gain: float32 [128], replicated, may hold values from 0.1 to 1.9
- out_weight: bfloat16 [2048, 2048], P('tp', 'kv'), may hold values from -0.125 to 0.125
- cache_keys: bfloat16 [16, 2048, 2, 128], P('dp', 'kv', 'tp'), may hold values from -400 to 400
- cache_values: bfloat16 [16, 2048, 2, 128], P('dp', 'kv', 'tp'), may hold values from -6 to 6
Outputs:
- mixed: bfloat16 [16, 2048], P('dp', 'kv')
- new_keys: bfloat16 [16, 2, 128], P('dp', 'tp')
- new_values: bfloat16 [16, 2, 128], P('dp', 'tp')
Inputs may be any that keep to these rules, and one draw needn't show every extreme that they name: `lengths`: of each index of dp's 8 sequences, the first has 1792 or more cached positions, the second fewer than 16, the others half of 2048 or more.
All inputs are finite; a program needn't handle non-finite values.
Results may differ from a plain program's by a relative error of at most 0.023.
Values may be sent and summed in bfloat16 or wider, within the bound.
A program may use at most 64 MiB of HBM per device.

v0:
```python
import math

import jax
import jax.numpy as jnp
from jax import lax
from jax.sharding import PartitionSpec as P

epsilon = 1e-06
rotary_base = 10000.0
masked_score = -1e30
output_scale = 0.2 + 0.6 * math.exp(-0.3)


def new_entries(proj_query, proj_key, proj_value, query_gain, key_gain, lengths):
    rows = proj_query.shape[0]
    head_dim = query_gain.shape[0]
    half_dim = head_dim // 2
    frequency = rotary_base ** (-jnp.arange(half_dim, dtype=jnp.float32) / half_dim)
    angle = lengths.astype(jnp.float32)[:, None, None, None] * frequency
    cosine_term = jnp.cos(angle)
    sine_term = jnp.sin(angle)

    def turned(pieces, gain):
        normed = (
            pieces * lax.rsqrt(jnp.mean(pieces * pieces, axis=-1, keepdims=True) + epsilon) * gain
        )
        lower_part = normed[..., :half_dim]
        upper_part = normed[..., half_dim:]
        return jnp.concatenate(
            [
                lower_part * cosine_term - upper_part * sine_term,
                upper_part * cosine_term + lower_part * sine_term,
            ],
            axis=-1,
        )

    queries = turned(proj_query.reshape(rows, -1, 2, head_dim), query_gain).astype(jnp.bfloat16)
    new_keys = turned(proj_key.reshape(rows, -1, 2, head_dim), key_gain).astype(jnp.bfloat16)
    new_values = proj_value.reshape(rows, -1, 2 * head_dim).astype(jnp.bfloat16)
    return (queries, new_keys.reshape(rows, -1, 2 * head_dim), new_values)


def body(
    tokens,
    lengths,
    query_weight,
    key_weight,
    value_weight,
    query_gain,
    key_gain,
    lambdas,
    head_gain,
    out_weight,
    cache_keys,
    cache_values,
):
    partial_query = jnp.dot(tokens, query_weight, preferred_element_type=jnp.float32)
    partial_key = jnp.dot(tokens, key_weight, preferred_element_type=jnp.float32)
    partial_value = jnp.dot(tokens, value_weight, preferred_element_type=jnp.float32)
    proj_query, proj_key, proj_value = lax.psum((partial_query, partial_key, partial_value), "kv")
    queries, new_keys, new_values = new_entries(
        proj_query, proj_key, proj_value, query_gain, key_gain, lengths
    )
    rows, positions, kv_heads, width = cache_keys.shape
    head_dim = width // 2
    scale = head_dim ** (-0.5)
    queries = queries.reshape(rows, kv_heads, -1, 2, head_dim)
    keys_split = cache_keys.reshape(rows, positions, kv_heads, 2, head_dim)
    scores = (
        jnp.einsum("skgtd,spktd->skgtp", queries, keys_split, preferred_element_type=jnp.float32)
        * scale
    )
    offset = lax.axis_index("kv") * positions
    position_ids = offset + jnp.arange(positions, dtype=jnp.int32)
    valid = (position_ids[None, :] < lengths[:, None])[:, None, None, None, :]
    local_highest = jnp.max(jnp.where(valid, scores, masked_score), axis=-1)
    highest = lax.pmax(local_highest, "kv")
    expo = jnp.where(valid, jnp.exp(scores - highest[..., None]), 0.0)
    totals = jnp.sum(expo, axis=-1)
    weighted = jnp.einsum(
        "skgtp,spke->skgte",
        expo.astype(jnp.bfloat16),
        cache_values,
        preferred_element_type=jnp.float32,
    )
    local_totals = totals
    local_weighted = weighted
    totals, weighted = lax.psum((local_totals, local_weighted), "kv")
    own_score = (
        jnp.einsum(
            "skgtd,sktd->skgt",
            queries,
            new_keys.reshape(rows, kv_heads, 2, head_dim),
            preferred_element_type=jnp.float32,
        )
        * scale
    )
    final_highest = jnp.maximum(highest, own_score)
    rescale = jnp.exp(highest - final_highest)
    own_weight = jnp.exp(own_score - final_highest)
    totals = totals * rescale + own_weight
    weighted = weighted * rescale[..., None]
    weighted = (
        weighted + own_weight[..., None] * new_values.astype(jnp.float32)[:, :, None, None, :]
    )
    heads = weighted / totals[..., None]
    gaps = heads[..., 0, :] - lambdas.reshape(kv_heads, -1)[None, :, :, None] * heads[..., 1, :]
    normed = gaps * lax.rsqrt(jnp.mean(gaps * gaps, axis=-1, keepdims=True) + epsilon) * head_gain
    attended = (normed * output_scale).astype(jnp.bfloat16).reshape(rows, -1)
    partial_out = jnp.dot(attended, out_weight, preferred_element_type=jnp.float32)
    mixed = lax.psum(partial_out.astype(jnp.bfloat16), "tp")
    return (mixed, new_keys, new_values)


def solution(mesh):
    return jax.shard_map(
        body,
        mesh=mesh,
        in_specs=(
            P("dp", "kv"),
            P("dp"),
            P("kv", "tp"),
            P("kv", "tp"),
            P("kv", "tp"),
            P(),
            P(),
            P("tp"),
            P(),
            P("tp", "kv"),
            P("dp", "kv", "tp", None),
            P("dp", "kv", "tp", None),
        ),
        out_specs=(P("dp", "kv"), P("dp", "tp", None), P("dp", "tp", None)),
        check_vma=False,
    )
```

profile of v0, /device:TPU:0, one launch (start us, length us, event | category | flops | bytes accessed | tf_op | source)
XLA Modules:
  0.0 148.0 jit_solution(14365525965118956070)
XLA Ops:
  7.2 0.0 copy-start
  7.2 0.0 copy-start.2
  7.2 0.0 all-reduce.3.cloned.1.call-start
  7.3 1.3 fusion.31
  8.6 0.1 reshape.286
  8.7 39.3 %psum.42 = f32[8,8,2,64]{3,1,2,0:T(8,128)S(1)} all-reduce(f32[8,8,2,64]{3,1,2,0:T(8,128)S(1)} %copy.29), channel_id=1, replica_groups=mesh['dp'=2,'kv'=8,'tp'=2] {'kv'}, use_global_device_ids=true, to_apply=%region_0.0 | all-reduce | flops 8192 | bytes 65536 | tf_op jit(solution)/shard_map/psum | solution.py:60
  48.0 0.1 multiply_reduce_fusion
  48.1 0.0 copy-start.9
  48.2 0.6 copy-done.9
  48.8 0.1 broadcast_compare_fusion
  48.9 0.0 copy-done.2
  48.9 0.0 copy-start.8
  48.9 0.2 copy.30
  49.1 0.4 copy-done.8
  49.5 0.1 multiply_multiply_fusion
  49.6 0.1 multiply_cosine_fusion
  49.7 0.1 subtract_convert_fusion
  49.8 0.3 select_reduce_fusion
  50.2 17.4 %pmax.7 = f32[8,1,8,2]{2,0,3,1:T(8,128)S(1)} all-reduce(f32[8,1,8,2]{2,0,3,1:T(8,128)S(1)} %bitcast.123), channel_id=1, replica_groups=mesh['dp'=2,'kv'=8,'tp'=2] {'kv'}, use_global_device_ids=true, to_apply=%region_3.0 | all-reduce | flops 128 | bytes 1024 | tf_op jit(solution)/shard_map/pmax | solution.py:77
  67.6 0.0 copy-done
  67.6 0.9 convolution_bitcast_fusion
  68.5 0.0 copy-start.3
  68.5 0.0 copy-start.5
  68.5 0.0 copy-start.4
  68.5 0.0 copy-start.11
  68.5 0.0 copy-start.6
  68.5 0.0 copy-start.10
  68.5 0.0 all-reduce.3.cloned.1.call-update
  68.5 0.0 copy-start.1
  68.5 0.2 fusion.2
  68.7 0.6 copy-done.3
  69.3 0.0 copy-done.5
  69.3 0.1 fusion.32
  69.4 0.1 reshape.290
  69.5 0.0 copy-done.4
  69.5 0.1 fusion.33
  69.6 34.9 %all-reduce = (f32[8,1,8,2]{2,0,3,1:T(8,128)S(1)}, f32[8,1,2,64]{3,2,0,1:T(2,128)S(1)}, bf16[8,128]{1,0:T(8,128)(2,1)S(1)}) all-reduce(f32[8,1,8,2]{2,0,3,1:T(8,128)S(1)} %bitcast.122, f32[8,1,2,64]{3,2,0,1:T(2,128)S(1)} %reshape.290, f32[8,128]{1,0:T(8,128)S(1)} %fusion.33), channel_id=1, replica_groups=mesh['dp'=2,'kv'=8,'tp'=2] {'kv'}, use_global_device_ids=true, to_apply=%region_9.10 | all-reduce | flops 2176 | bytes 15360 | tf_op jit(solution)/shard_map/psum | solution.py:88
  104.5 0.0 copy-start.7
  104.5 0.1 multiply_reduce_fusion.1
  104.6 0.0 copy-done.11
  104.7 0.1 multiply_multiply_fusion.1
  104.7 0.1 subtract_convert_fusion.1
  104.8 0.1 maximum_bitcast_fusion
  104.9 0.2 fusion.23
  105.1 0.0 copy-done.6
  105.1 0.0 copy-done.10
  105.2 0.1 broadcast_bitcast_fusion
  105.2 0.1 pad_maximum_fusion.3
  105.3 0.7 convert_element_type.49
  106.0 0.0 copy-done.7
  106.0 30.7 %all-reduce.3.cloned.1.call-done = f32[8,1,8,2,128]{4,2,3,0,1:T(8,128)} async-done(((f32[8,1,8,2,128]{4,2,3,0,1:T(8,128)}), f32[8,1,8,2,128]{4,2,3,0,1:T(8,128)}) %all-reduce.3.cloned.1.call-update) | async-done | bytes 65552 | tf_op jit(solution)/shard_map/psum | solution.py:88
  136.7 1.0 add_divide_fusion
  137.7 0.2 fusion.15
  137.8 0.1 copy.38
  137.9 0.0 copy-done.1
  137.9 0.2 convolution_convert_fusion
  138.1 3.0 %psum.47 = bf16[8,256]{1,0:T(8,128)(2,1)} all-reduce(bf16[8,256]{1,0:T(8,128)(2,1)S(1)} %convolution_convert_fusion), channel_id=1, replica_groups=mesh['dp'=2,'kv'=8,'tp'=2] {'tp'}, use_global_device_ids=true, to_apply=%region_11.12 | all-reduce | flops 2048 | bytes 8192 | tf_op jit(solution)/shard_map/psum | solution.py:111
  (16 shorter events, 0.1 us)
Async XLA Ops:
  7.2 60.4 %copy-start = (bf16[8,256,1,128]{3,1,2,0:T(8,128)(2,1)S(1)}, bf16[8,256,1,128]{3,1,2,0:T(8,128)(2,1)}, u32[]{:S(2)}) copy-start(bf16[8,256,1,128]{3,1,2,0:T(8,128)(2,1)} %param.23) | copy-start | bytes 1572868
  7.2 41.7 %copy-start.2 = (bf16[8,256,1,128]{3,1,2,0:T(8,128)(2,1)S(1)}, bf16[8,256,1,128]{3,1,2,0:T(8,128)(2,1)}, u32[]{:S(2)}) copy-start(bf16[8,256,1,128]{3,1,2,0:T(8,128)(2,1)} %param.22) | copy-start | bytes 1572868
  7.2 129.5 %all-reduce.3.cloned.1.call-start = ((), (), s32[]{:S(2)}) async-start(), calls=%async_computation | async-start | bytes 131072 | tf_op jit(solution)/shard_map/psum | solution.py:88
  48.1 0.7 copy-start.9
  48.9 0.7 copy-start.8
  68.5 0.8 copy-start.3
  68.5 0.8 copy-start.5
  68.5 1.0 copy-start.4
  68.5 36.2 %copy-start.11 = (f32[64]{0:T(128)S(1)}, f32[64]{0:T(128)}, u32[]{:S(2)}) copy-start(f32[64]{0:T(128)} %param.18) | copy-start | bytes 772
  68.5 36.7 %copy-start.6 = (f32[8]{0:T(128)S(1)}, f32[8]{0:T(128)}, u32[]{:S(2)}) copy-start(f32[8]{0:T(128)} %param.19) | copy-start | bytes 100
  68.5 36.7 %copy-start.10 = (f32[128]{0:T(128)S(1)}, f32[128]{0:T(128)}, u32[]{:S(2)}) copy-start(f32[128]{0:T(128)} %param.20) | copy-start | bytes 1540
  68.5 69.4 %copy-start.1 = (bf16[1024,256]{1,0:T(8,128)(2,1)S(1)}, bf16[1024,256]{1,0:T(8,128)(2,1)}, u32[]{:S(2)}) copy-start(bf16[1024,256]{1,0:T(8,128)(2,1)} %param.21) | copy-start | bytes 1572868
  104.5 1.5 copy-start.7
Sparse Core Ops, SparseCore 0:
  68.6 67.9 all-reduce.2
where the time goes:
time: 148 us
  blocking collectives  94.7 us (64%)
  waiting for transfers between devices  30.7 us (21%)
  between operations  14.3 us (10%)
  matrix products  3.2 us (2%)
  local copies, waits for them, and re-layouts  2.93 us (2%)
  other arithmetic  2.22 us (2%)
    psum x1, blocking collectives, body(): lax.psum((partial_query, partial_key, partial_value), 'kv')  39.3 us
    psum x1, blocking collectives, body(): totals, weighted = lax.psum((local_totals, local_weighted), 'kv')  34.9 us
    psum x1, waiting for transfers between devices, body(): totals, weighted = lax.psum((local_totals, local_weighted), 'kv')  30.7 us
    pmax x1, blocking collectives, body(): highest = lax.pmax(local_highest, 'kv')  17.4 us
    psum x1, blocking collectives, body(): mixed = lax.psum(partial_out.astype(jnp.bfloat16), 'tp')  3.05 us
  transfers between devices with their start and end apart: 1, of which 1 were waited for; matrix products, arithmetic and copies ran while one was open for 1% of the time, Pallas kernels for 0%

commit v1 on v0

v1 whole, which is shorter than its diff:
```python
import functools
import math

import jax
import jax.numpy as jnp
import numpy as np
from jax import lax
from jax.experimental import pallas as pl
from jax.experimental.pallas import tpu as pltpu
from jax.sharding import PartitionSpec as P

epsilon = 1e-06
rotary_base = 10000.0
masked_score = -1e30
output_scale = 0.2 + 0.6 * math.exp(-0.3)
unroll_limit = 16
f32 = jnp.float32
bf16 = jnp.bfloat16
MESH = pl.DeviceIdType.MESH


def over(lo, hi, step):
    if hi - lo <= unroll_limit:
        for i in range(lo, hi):
            step(i)
    else:

        def one(i, carry):
            step(i)
            return carry

        lax.fori_loop(lo, hi, one, 0)


def gather(n, step, init):
    if n <= unroll_limit:
        for i in range(n):
            init = step(i, init)
        return init
    return lax.fori_loop(0, n, step, init)


def kernel(
    n_kv,
    n_tp,
    lengths,
    lambdas,
    tokens_h,
    wq_h,
    wk_h,
    wv_h,
    freq_h,
    qg_h,
    kg_h,
    hg_h,
    wo_h,
    ck_h,
    cv_h,
    mixed_o,
    nk_o,
    nv_o,
    tokens,
    wq,
    wk,
    wv,
    freq,
    qg,
    kg,
    hg,
    wo,
    ck,
    cv,
    send_a,
    recv_a,
    wide,
    qbuf,
    send_w,
    send_s,
    recv_w,
    recv_s,
    att,
    att_f,
    part,
    load_sem,
    a_send,
    a_recv,
    b_send,
    b_recv,
    w_send,
    w_recv,
    s_send,
    s_recv,
    e_send,
    e_recv,
    t_send,
    t_recv,
):
    me = lax.axis_index("kv")
    core = lax.axis_index("tp")
    rows, positions, width = ck.shape
    half = width // 2
    quarter = half // 2
    heads = wq.shape[1] // width
    slab = heads + 2
    owners = min(n_kv, rows)
    owned = rows // owners
    scale = half ** (-0.5)

    pairs = [
        (tokens_h, tokens),
        (wq_h, wq),
        (wk_h, wk),
        (wv_h, wv),
        (freq_h, freq),
        (qg_h, qg),
        (kg_h, kg),
        (hg_h, hg),
        (ck_h, ck),
        (cv_h, cv),
        (wo_h, wo),
    ]
    loads = [
        pltpu.make_async_copy(src, dst, load_sem.at[i]) for i, (src, dst) in enumerate(pairs)
    ]
    for load in loads:
        load.start()

    barrier = pltpu.get_barrier_semaphore()

    def peer_of(o):
        return lax.rem(me + o, n_kv)

    def greet(o):
        pl.semaphore_signal(barrier, inc=1, device_id={"kv": peer_of(o)}, device_id_type=MESH)

    over(1, n_kv, greet)
    for o in range(1, n_tp):
        pl.semaphore_signal(
            barrier, inc=1, device_id={"tp": lax.rem(core + o, n_tp)}, device_id_type=MESH
        )

    def if_owner(index, run):
        if owners == n_kv:
            run()
        else:
            pl.when(index < owners)(run)

    def remote(src, dst, ssem, rsem, peer):
        return pltpu.make_async_remote_copy(
            src_ref=src,
            dst_ref=dst,
            send_sem=ssem,
            recv_sem=rsem,
            device_id={"kv": peer},
            device_id_type=MESH,
        )

    def rows_of(index):
        return pl.ds(index * owned, owned)

    for load in loads[:4]:
        load.wait()
    x = tokens[...]
    pq = jnp.dot(x, wq[...], preferred_element_type=f32)
    pk = jnp.dot(x, wk[...], preferred_element_type=f32)
    pv = jnp.dot(x, wv[...], preferred_element_type=f32)
    for h in range(heads):
        send_a[:, h, :] = pq[:, h * width : (h + 1) * width]
    send_a[:, heads, :] = pk
    send_a[:, heads + 1, :] = pv

    pl.semaphore_wait(barrier, n_kv - 1 + n_tp - 1)

    def copy_a(peer):
        return remote(
            send_a.at[rows_of(peer)], recv_a.at[me], a_send.at[peer], a_recv.at[me], peer
        )

    def start_a(o):
        peer = peer_of(o)
        if_owner(peer, lambda: copy_a(peer).start())

    over(1, n_kv, start_a)

    lane = lax.broadcasted_iota(jnp.int32, (1, width), 1)
    low_map = lane < half
    low_half = lax.rem(lane, half) < quarter
    eye = lax.broadcasted_iota(jnp.int32, (2 * heads, width), 0) == lax.broadcasted_iota(
        jnp.int32, (2 * heads, width), 1
    )

    def to_lanes(column):
        return jnp.sum(jnp.where(eye, column, 0.0), axis=0, keepdims=True)

    def to_column(line):
        return jnp.sum(jnp.where(eye, line, 0.0), axis=1, keepdims=True)

    for load in loads[4:8]:
        load.wait()

    def own_a():
        gain_q = jnp.concatenate([qg[...], qg[...]], axis=1)
        gain_k = jnp.concatenate([kg[...], kg[...]], axis=1)
        slab_row = lax.broadcasted_iota(jnp.int32, (slab, width), 0)
        gain = jnp.where(slab_row < heads, gain_q, gain_k)
        turns = []
        for j in range(owned):
            angle = lengths[me * owned + j].astype(f32) * freq[...]
            turns.append((jnp.cos(angle), jnp.where(low_half, -1.0, 1.0) * jnp.sin(angle)))
        recv_a[pl.ds(me, 1)] = send_a[rows_of(me)][None]

        def wait_a(o):
            peer = peer_of(o)
            remote(
                send_a.at[rows_of(0)], recv_a.at[peer], a_send.at[0], a_recv.at[peer], peer
            ).wait_recv()

        over(1, n_kv, wait_a)
        wide[...] = jnp.zeros_like(wide)
        for j in range(owned):
            total = gather(n_kv, lambda i, t: t + recv_a[i, j], jnp.zeros((slab, width), f32))
            square = total * total
            mean_lo = jnp.sum(jnp.where(low_map, square, 0.0), axis=1, keepdims=True)
            mean_hi = jnp.sum(jnp.where(low_map, 0.0, square), axis=1, keepdims=True)
            mean = jnp.where(low_map, mean_lo, mean_hi) * (1.0 / half)
            normed = total * lax.rsqrt(mean + epsilon) * gain
            other = jnp.where(
                low_half,
                pltpu.roll(normed, width - quarter, 1),
                pltpu.roll(normed, quarter, 1),
            )
            cosine, sine = turns[j]
            turned = normed * cosine + other * sine
            wide[:slab, :] = jnp.where(slab_row <= heads, turned, total)
            qbuf[pl.ds(me * owned + j, 1)] = wide[...].astype(bf16)[None]

    if_owner(me, own_a)

    def copy_b(peer):
        mine = qbuf.at[rows_of(me)]
        return remote(mine, mine, b_send.at[peer], b_recv.at[me], peer)

    if_owner(me, lambda: over(1, n_kv, lambda o: copy_b(peer_of(o)).start()))

    def arrived(buf, sem):
        def wait(o):
            peer = peer_of(o)

            def run():
                theirs = buf.at[rows_of(peer)]
                remote(theirs, theirs, b_send.at[0], sem.at[peer], peer).wait_recv()

            if_owner(peer, run)

        over(1, n_kv, wait)

    loads[8].wait()
    loads[9].wait()
    arrived(qbuf, b_recv)

    place = me * positions + lax.broadcasted_iota(jnp.int32, (1, positions), 1)
    for s in range(rows):
        q = qbuf[s][:heads].astype(f32)
        both = jnp.concatenate(
            [jnp.where(low_map, q, 0.0), jnp.where(low_map, 0.0, q)], axis=0
        ).astype(bf16)
        scores = (
            lax.dot_general(both, ck[s], (((1,), (1,)), ((), ())), preferred_element_type=f32)
            * scale
        )
        valid = place < lengths[s]
        highest = jnp.max(jnp.where(valid, scores, masked_score), axis=1, keepdims=True)
        expo = jnp.where(valid, jnp.exp(scores - highest), 0.0)
        send_s[s, 0:1, :] = to_lanes(highest)
        send_s[s, 1:2, :] = to_lanes(jnp.sum(expo, axis=1, keepdims=True))
        send_w[s] = jnp.dot(expo.astype(bf16), cv[s], preferred_element_type=f32)

    def copy_w(peer):
        return remote(
            send_w.at[rows_of(peer)], recv_w.at[me], w_send.at[peer], w_recv.at[me], peer
        )

    def copy_s(peer):
        return remote(
            send_s.at[rows_of(peer)], recv_s.at[me], s_send.at[peer], s_recv.at[me], peer
        )

    def start_d(o):
        peer = peer_of(o)

        def run():
            copy_s(peer).start()
            copy_w(peer).start()

        if_owner(peer, run)

    over(1, n_kv, start_d)

    nk_o[...] = jnp.concatenate(
        [qbuf[s].astype(f32)[heads : heads + 1] for s in range(rows)], axis=0
    ).astype(bf16)
    nv_o[...] = jnp.concatenate(
        [qbuf[s].astype(f32)[heads + 1 : heads + 2] for s in range(rows)], axis=0
    ).astype(bf16)

    def own_d():
        recv_w[pl.ds(me, 1)] = send_w[rows_of(me)][None]
        recv_s[pl.ds(me, 1)] = send_s[rows_of(me)][None]
        weigh = jnp.where(lane < heads, 1.0, 0.0)
        for h in range(heads):
            weigh = jnp.where(lane == heads + h, -lambdas[h], weigh)
        owns = []
        for j in range(owned):
            entry = qbuf[pl.ds(me * owned + j, 1)][0].astype(f32)
            dots = entry[:heads] * entry[heads : heads + 1]
            own_lo = jnp.sum(jnp.where(low_map, dots, 0.0), axis=1, keepdims=True)
            own_hi = jnp.sum(jnp.where(low_map, 0.0, dots), axis=1, keepdims=True)
            own = to_lanes(jnp.concatenate([own_lo, own_hi], axis=0) * scale)
            owns.append((own, entry[heads + 1 : heads + 2]))

        def wait_s(o):
            peer = peer_of(o)
            remote(
                send_s.at[rows_of(0)], recv_s.at[peer], s_send.at[0], s_recv.at[peer], peer
            ).wait_recv()

        def wait_w(o):
            peer = peer_of(o)
            remote(
                send_w.at[rows_of(0)], recv_w.at[peer], w_send.at[0], w_recv.at[peer], peer
            ).wait_recv()

        over(1, n_kv, wait_s)
        over(1, n_kv, wait_w)
        for j in range(owned):
            own, new_value = owns[j]
            highest = gather(n_kv, lambda i, m: jnp.maximum(m, recv_s[i, j, 0:1, :]), own)
            own_weight = jnp.exp(own - highest)
            total = gather(
                n_kv,
                lambda i, t: t
                + recv_s[i, j, 1:2, :] * jnp.exp(recv_s[i, j, 0:1, :] - highest),
                own_weight,
            )
            share = weigh / total
            heads_sum = gather(
                n_kv,
                lambda i, t: t
                + recv_w[i, j] * to_column(share * jnp.exp(recv_s[i, j, 0:1, :] - highest)),
                to_column(share * own_weight) * new_value,
            )
            gaps = heads_sum[:heads] + heads_sum[heads:]
            mean = jnp.mean(gaps * gaps, axis=1, keepdims=True)
            normed = gaps * lax.rsqrt(mean + epsilon) * hg[...]
            att[pl.ds(me * owned + j, 1)] = (normed * output_scale).astype(bf16)[None]

    if_owner(me, own_d)

    def copy_e(peer):
        mine = att.at[rows_of(me)]
        return remote(mine, mine, e_send.at[peer], e_recv.at[me], peer)

    if_owner(me, lambda: over(1, n_kv, lambda o: copy_e(peer_of(o)).start()))
    loads[10].wait()
    arrived(att, e_recv)

    att_f[...] = att[...].astype(f32).reshape(rows * heads, width)
    attended = jnp.concatenate(
        [att_f[pl.ds(h, rows, stride=heads), :] for h in range(heads)], axis=1
    ).astype(bf16)
    part[pl.ds(core, 1)] = jnp.dot(attended, wo[...], preferred_element_type=f32).astype(bf16)[
        None
    ]

    def copy_t(peer):
        return pltpu.make_async_remote_copy(
            src_ref=part.at[core],
            dst_ref=part.at[core],
            send_sem=t_send.at[peer],
            recv_sem=t_recv.at[core],
            device_id={"tp": peer},
            device_id_type=MESH,
        )

    for o in range(1, n_tp):
        copy_t(lax.rem(core + o, n_tp)).start()
    for o in range(1, n_tp):
        peer = lax.rem(core + o, n_tp)
        pltpu.make_async_remote_copy(
            src_ref=part.at[peer],
            dst_ref=part.at[peer],
            send_sem=t_send.at[0],
            recv_sem=t_recv.at[peer],
            device_id={"tp": peer},
            device_id_type=MESH,
        ).wait_recv()
    mixed_o[...] = gather(
        n_tp, lambda i, t: t + part[i].astype(f32), jnp.zeros(mixed_o.shape, f32)
    ).astype(bf16)

    def sent(o):
        peer = peer_of(o)

        def run():
            copy_a(peer).wait_send()
            copy_s(peer).wait_send()
            copy_w(peer).wait_send()

        if_owner(peer, run)

    def sent_all(o):
        peer = peer_of(o)
        copy_b(peer).wait_send()
        copy_e(peer).wait_send()

    over(1, n_kv, sent)
    if_owner(me, lambda: over(1, n_kv, sent_all))
    for o in range(1, n_tp):
        copy_t(lax.rem(core + o, n_tp)).wait_send()


def body(
    n_kv,
    n_tp,
    tokens,
    lengths,
    query_weight,
    key_weight,
    value_weight,
    query_gain,
    key_gain,
    lambdas,
    head_gain,
    out_weight,
    cache_keys,
    cache_values,
):
    rows, positions, kv_heads, width = cache_keys.shape
    assert kv_heads == 1 and key_weight.shape[1] == width
    half = width // 2
    quarter = half // 2
    heads = query_weight.shape[1] // width
    owners = min(n_kv, rows)
    assert rows % owners == 0
    owned = rows // owners
    ck = cache_keys.reshape(rows, positions, width)
    cv = cache_values.reshape(rows, positions, width)
    exponent = -(np.arange(width) % quarter) / quarter
    freq = jnp.asarray((rotary_base**exponent).astype(np.float32)[None])
    qg = query_gain.reshape(1, half)
    kg = key_gain.reshape(1, half)
    hg = head_gain.reshape(1, width)
    held = [
        tokens,
        query_weight,
        key_weight,
        value_weight,
        freq,
        qg,
        kg,
        hg,
        out_weight,
        ck,
        cv,
    ]
    dma = pltpu.SemaphoreType.DMA
    smem = pl.BlockSpec(memory_space=pltpu.SMEM)
    hbm = pl.BlockSpec(memory_space=pl.ANY)
    vmem = pl.BlockSpec(memory_space=pltpu.VMEM)
    out_columns = out_weight.shape[1]
    wide_rows = -(-(heads + 2) // 16) * 16
    mixed, new_keys, new_values = pl.pallas_call(
        functools.partial(kernel, n_kv, n_tp),
        name="decode_step",
        out_shape=[
            jax.ShapeDtypeStruct((rows, out_columns), bf16),
            jax.ShapeDtypeStruct((rows, width), bf16),
            jax.ShapeDtypeStruct((rows, width), bf16),
        ],
        in_specs=[smem, smem] + [hbm] * len(held),
        out_specs=[vmem] * 3,
        scratch_shapes=[pltpu.VMEM(a.shape, a.dtype) for a in held]
        + [
            pltpu.VMEM((rows, heads + 2, width), f32),
            pltpu.VMEM((n_kv, owned, heads + 2, width), f32),
            pltpu.VMEM((wide_rows, width), f32),
            pltpu.VMEM((rows, wide_rows, width), bf16),
            pltpu.VMEM((rows, 2 * heads, width), f32),
            pltpu.VMEM((rows, 2, width), f32),
            pltpu.VMEM((n_kv, owned, 2 * heads, width), f32),
            pltpu.VMEM((n_kv, owned, 2, width), f32),
            pltpu.VMEM((rows, heads, width), bf16),
            pltpu.VMEM((rows * heads, width), f32),
            pltpu.VMEM((n_tp, rows, out_columns), bf16),
            dma((len(held),)),
            dma((owners,)),
            dma((n_kv,)),
            dma((n_kv,)),
            dma((owners,)),
            dma((owners,)),
            dma((n_kv,)),
            dma((owners,)),
            dma((n_kv,)),
            dma((n_kv,)),
            dma((owners,)),
            dma((n_tp,)),
            dma((n_tp,)),
        ],
        compiler_params=pltpu.CompilerParams(collective_id=0, has_side_effects=True),
    )(lengths, lambdas, *held)
    return (
        mixed,
        new_keys.reshape(rows, kv_heads, width),
        new_values.reshape(rows, kv_heads, width),
    )


def solution(mesh):
    return jax.shard_map(
        functools.partial(body, mesh.shape["kv"], mesh.shape["tp"]),
        mesh=mesh,
        in_specs=(
            P("dp", "kv"),
            P("dp"),
            P("kv", "tp"),
            P("kv", "tp"),
            P("kv", "tp"),
            P(),
            P(),
            P("tp"),
            P(),
            P("tp", "kv"),
            P("dp", "kv", "tp", None),
            P("dp", "kv", "tp", None),
        ),
        out_specs=(P("dp", "kv"), P("dp", "tp", None), P("dp", "tp", None)),
        check_vma=False,
    )
```

time: 148 us -> 31.8 us (0.21)
  blocking collectives: 94.7 us -> 0 us
  waiting for transfers between devices: 30.7 us -> 0 us
  Pallas kernels: 0 us -> 28.3 us
  between operations: 14.3 us -> 0.65 us
  matrix products: 3.2 us -> 0 us
  other arithmetic: 2.22 us -> 0 us
    psum x3 -> x0, blocking collectives: 77.3 us -> none  [the longest x1 39.3 us: body(): lax.psum((partial_query, partial_key, partial_value), 'kv')]
    psum x1 -> x0, waiting for transfers between devices: 30.7 us -> none  [body(): totals, weighted = lax.psum((local_totals, local_weighted), 'kv')]
    pallas_call x0 -> x1, Pallas kernels: none -> 28.3 us  [body(): pl.pallas_call(functools.partial(kernel, n_kv, n_tp), name='decode_step',...]
    pmax x1 -> x0, blocking collectives: 17.4 us -> none  [body(): highest = lax.pmax(local_highest, 'kv')]
    dot_general x7 -> x0, matrix products: 3.2 us -> none  [the longest x1 1.34 us: body(): jnp.dot(tokens, query_weight, preferred_element_type=jnp.float32)]
  transfers between devices with their start and end apart: 1 -> 0, of which waited for: 1 -> 0; matrix products, arithmetic and copies ran while one was open for 1% -> 0% of each run, Pallas kernels for 0% -> 0%
where the time goes in v1:
time: 31.8 us; the launch traced here: 31.5 us
  Pallas kernels  28.3 us (89%)
  local copies, waits for them, and re-layouts  2.59 us (8%)
  between operations  0.65 us (2%)
    pallas_call x1, Pallas kernels, body(): pl.pallas_call(functools.partial(kernel, n_kv, n_tp), name='decode_step',...  28.3 us
    unnamed x9, local copies, waits for them, and re-layouts  2.59 us

profile of v1, /device:TPU:0, one launch (start us, length us, event | category | flops | bytes accessed | tf_op | source)
XLA Modules:
  0.0 31.5 jit_solution(15575986672447948328)
XLA Ops:
  0.6 28.3 %decode_step.1 = (bf16[8,256]{1,0:T(8,128)(2,1)}, bf16[8,128]{1,0:T(8,128)(2,1)}, bf16[8,128]{1,0:T(8,128)(2,1)}) custom-call(s32[8]{0:T(128)} %lengths.1, f32[8]{0:T(128)} %lambdas.1, bf16[8,256]{1,0:T(8,128)(2,1)} %tokens_h.1, bf16[256,1024]{1,0:T(8,128)(2,1)} %wq_h.1, bf16[256,128]{1,0:T(8,128)(2,1)} %wk_h.1, bf16[256,128]{1,0:T(8,128)(2,1)} %wv_h.1, ...), custom_call_target="tpu_custom_call" | custom-call | tf_op jit(solution)/shard_map/decode_step/pallas_call | solution.py:472
  28.9 0.0 copy-start
  28.9 0.7 %copy-done = bf16[8,256]{1,0:T(8,128)(2,1)S(1)} copy-done((bf16[8,256]{1,0:T(8,128)(2,1)S(1)}, bf16[8,256]{1,0:T(8,128)(2,1)}, u32[]{:S(2)}) %copy-start) | copy-done | bytes 4120
  29.6 0.0 copy-start.2
  29.6 0.6 %copy.19 = bf16[8,256]{1,0:T(8,128)(2,1)} copy(bf16[8,256]{1,0:T(8,128)(2,1)S(1)} %copy-done) | data formatting | bytes 8192
  30.2 0.1 copy-done.2
  30.3 0.0 copy-start.1
  30.3 0.6 %copy.20 = bf16[8,1,128]{2,0,1:T(8,128)(2,1)} copy(bf16[8,1,128]{2,0,1:T(8,128)(2,1)S(1)} %bitcast.10) | data formatting | bytes 4096
  30.9 0.1 copy-done.1
  31.0 0.6 %copy.21 = bf16[8,1,128]{2,0,1:T(8,128)(2,1)} copy(bf16[8,1,128]{2,0,1:T(8,128)(2,1)S(1)} %bitcast.9) | data formatting | bytes 4096
Async XLA Ops:
  28.9 0.7 %copy-start = (bf16[8,256]{1,0:T(8,128)(2,1)S(1)}, bf16[8,256]{1,0:T(8,128)(2,1)}, u32[]{:S(2)}) copy-start(bf16[8,256]{1,0:T(8,128)(2,1)} %get-tuple-element.12) | copy-start | bytes 12292
  29.6 0.7 %copy-start.2 = (bf16[8,128]{1,0:T(8,128)(2,1)S(1)}, bf16[8,128]{1,0:T(8,128)(2,1)}, u32[]{:S(2)}) copy-start(bf16[8,128]{1,0:T(8,128)(2,1)} %get-tuple-element.7) | copy-start | bytes 6148
  30.3 0.7 %copy-start.1 = (bf16[8,128]{1,0:T(8,128)(2,1)S(1)}, bf16[8,128]{1,0:T(8,128)(2,1)}, u32[]{:S(2)}) copy-start(bf16[8,128]{1,0:T(8,128)(2,1)} %get-tuple-element.8) | copy-start | bytes 6148

commit v2 on v1

v2 whole, which is shorter than its diff:
```python
import functools
import math

import jax
import jax.numpy as jnp
import numpy as np
from jax import lax
from jax.experimental import pallas as pl
from jax.experimental.pallas import tpu as pltpu
from jax.sharding import PartitionSpec as P

epsilon = 1e-06
rotary_base = 10000.0
masked_score = -1e30
output_scale = 0.2 + 0.6 * math.exp(-0.3)
unroll_limit = 16
f32 = jnp.float32
bf16 = jnp.bfloat16
MESH = pl.DeviceIdType.MESH


def over(lo, hi, step):
    if hi - lo <= unroll_limit:
        for i in range(lo, hi):
            step(i)
    else:

        def one(i, carry):
            step(i)
            return carry

        lax.fori_loop(lo, hi, one, 0)


def gather(n, step, init):
    if n <= unroll_limit:
        for i in range(n):
            init = step(i, init)
        return init
    return lax.fori_loop(0, n, step, init)


def kernel(
    n_kv,
    n_tp,
    lengths_h,
    lambdas_h,
    tokens_h,
    wq_h,
    wk_h,
    wv_h,
    freq_h,
    qg_h,
    kg_h,
    hg_h,
    ck_h,
    cv_h,
    wo_h,
    mixed_o,
    nk_o,
    nv_o,
    lengths,
    lambdas,
    tokens,
    wq,
    wk,
    wv,
    freq,
    qg,
    kg,
    hg,
    ck,
    cv,
    wo,
    send_a,
    recv_a,
    send_n,
    recv_n,
    qbuf,
    nbuf,
    send_w,
    send_s,
    recv_w,
    recv_s,
    att,
    att_f,
    load_sem,
    a_send,
    a_recv,
    n_send,
    n_recv,
    b_send,
    b_recv,
    k_send,
    k_recv,
    w_send,
    w_recv,
    s_send,
    s_recv,
    e_send,
    e_recv,
    o_send,
    o_recv,
):
    me = lax.axis_index("kv")
    core = lax.axis_index("tp")
    rows, positions, width = ck.shape
    half = width // 2
    quarter = half // 2
    heads = wq.shape[1] // width
    owners, owned, base = owner_plan(n_kv, rows)
    mine = me - base
    is_owner = jnp.logical_and(me >= base, me < base + owners)
    scale = half ** (-0.5)

    pairs = [
        (tokens_h, tokens),
        (wq_h, wq),
        (wk_h, wk),
        (wv_h, wv),
        (lengths_h, lengths),
        (freq_h, freq),
        (qg_h, qg),
        (kg_h, kg),
        (hg_h, hg),
        (lambdas_h, lambdas),
        (ck_h, ck),
        (cv_h, cv),
        (wo_h, wo.at[core]),
    ]
    loads = [
        pltpu.make_async_copy(src, dst, load_sem.at[i]) for i, (src, dst) in enumerate(pairs)
    ]

    barrier = pltpu.get_barrier_semaphore()

    def greet(peer, other):
        pl.semaphore_signal(
            barrier, inc=1, device_id={"kv": peer, "tp": other}, device_id_type=MESH
        )

    def cores():
        return [(lax.rem(core + c, n_tp), c) for c in range(n_tp)]

    def peer_of(o):
        return lax.rem(me + o, n_kv)

    @pl.when(is_owner)
    def _():
        for other, c in cores():
            over(0 if c else 1, n_kv, lambda o: greet(peer_of(o), other))

    @pl.when(jnp.logical_not(is_owner))
    def _():
        for other, c in cores():
            over(0, owners, lambda g: greet(base + g, other))
            if c:
                greet(me, other)

    for load in loads:
        load.start()

    def remote(src, dst, ssem, rsem, peer, other=None):
        return pltpu.make_async_remote_copy(
            src_ref=src,
            dst_ref=dst,
            send_sem=ssem,
            recv_sem=rsem,
            device_id={"kv": peer, "tp": core if other is None else other},
            device_id_type=MESH,
        )

    def rows_of(group):
        return pl.ds(group * owned, owned)

    for load in loads[:4]:
        load.wait()
    x = tokens[...]
    pq = jnp.dot(x, wq[...], preferred_element_type=f32)
    pk = jnp.dot(x, wk[...], preferred_element_type=f32)
    pv = jnp.dot(x, wv[...], preferred_element_type=f32)
    for h in range(heads):
        send_a[:, h, :] = pq[:, h * width : (h + 1) * width]
    send_n[:, 0, :] = pk
    send_n[:, 1, :] = pv

    @pl.when(is_owner)
    def _():
        pl.semaphore_wait(barrier, n_kv * n_tp - 1)

    @pl.when(jnp.logical_not(is_owner))
    def _():
        pl.semaphore_wait(barrier, owners * n_tp + n_tp - 1)

    def copy_a(g):
        return remote(send_a.at[rows_of(g)], recv_a.at[me], a_send.at[g], a_recv.at[me], base + g)

    def copy_n(g):
        return remote(send_n.at[rows_of(g)], recv_n.at[me], n_send.at[g], n_recv.at[me], base + g)

    upper = (2 * me) // n_kv

    def near(t):
        return t + upper * (owners - 1 - 2 * t)

    def start_a(t):
        g = near(owners - 1 - t)

        @pl.when(base + g != me)
        def _():
            copy_a(g).start()
            copy_n(g).start()

    over(0, owners, start_a)

    def copy_o(other):
        return remote(wo_h, wo.at[core], o_send.at[other], o_recv.at[core], me, other)

    for other, c in cores():
        if c:
            copy_o(other).start()

    lane = lax.broadcasted_iota(jnp.int32, (1, width), 1)
    low_map = lane < half
    low_half = lax.rem(lane, half) < quarter
    eye = lax.broadcasted_iota(jnp.int32, (2 * heads, width), 0) == lax.broadcasted_iota(
        jnp.int32, (2 * heads, width), 1
    )

    def to_lanes(column):
        return jnp.sum(jnp.where(eye, column, 0.0), axis=0, keepdims=True)

    def to_column(line):
        return jnp.sum(jnp.where(eye, line, 0.0), axis=1, keepdims=True)

    for load in loads[4:10]:
        load.wait()

    def copy_b(peer):
        ref = qbuf.at[rows_of(mine)]
        return remote(ref, ref, b_send.at[peer], b_recv.at[mine], peer)

    def copy_k(peer):
        ref = nbuf.at[rows_of(mine)]
        return remote(ref, ref, k_send.at[peer], k_recv.at[mine], peer)

    @pl.when(is_owner)
    def _():
        gain_q = jnp.concatenate([qg[...], qg[...]], axis=1)
        gain_k = jnp.concatenate([kg[...], kg[...]], axis=1)
        turns = []
        for j in range(owned):
            angle = lengths[mine * owned + j].astype(f32) * freq[...]
            turns.append((jnp.cos(angle), jnp.where(low_half, -1.0, 1.0) * jnp.sin(angle)))
        recv_a[pl.ds(me, 1)] = send_a[rows_of(mine)][None]
        recv_n[pl.ds(me, 1)] = send_n[rows_of(mine)][None]

        def turned(total, gain, turn):
            square = total * total
            mean_lo = jnp.sum(jnp.where(low_map, square, 0.0), axis=1, keepdims=True)
            mean_hi = jnp.sum(jnp.where(low_map, 0.0, square), axis=1, keepdims=True)
            mean = jnp.where(low_map, mean_lo, mean_hi) * (1.0 / half)
            normed = total * lax.rsqrt(mean + epsilon) * gain
            other = jnp.where(
                low_half,
                pltpu.roll(normed, width - quarter, 1),
                pltpu.roll(normed, quarter, 1),
            )
            return normed * turn[0] + other * turn[1]

        def wait_a(o):
            peer = peer_of(o)
            remote(
                send_a.at[rows_of(0)], recv_a.at[peer], a_send.at[0], a_recv.at[peer], peer
            ).wait_recv()

        def wait_n(o):
            peer = peer_of(o)
            remote(
                send_n.at[rows_of(0)], recv_n.at[peer], n_send.at[0], n_recv.at[peer], peer
            ).wait_recv()

        over(1, n_kv, wait_a)
        for j in range(owned):
            total = gather(n_kv, lambda i, t: t + recv_a[i, j], jnp.zeros((heads, width), f32))
            qbuf[pl.ds(mine * owned + j, 1)] = turned(total, gain_q, turns[j]).astype(bf16)[None]
        over(1, n_kv, lambda o: copy_b(peer_of(o)).start())
        over(1, n_kv, wait_n)
        first = lax.broadcasted_iota(jnp.int32, (2, width), 0) == 0
        for j in range(owned):
            total = gather(n_kv, lambda i, t: t + recv_n[i, j], jnp.zeros((2, width), f32))
            entry = jnp.where(first, turned(total, gain_k, turns[j]), total)
            nbuf[pl.ds(mine * owned + j, 1)] = entry.astype(bf16)[None]
        over(1, n_kv, lambda o: copy_k(peer_of(o)).start())

    def arrive(buf, sem, g):
        ref = buf.at[rows_of(g)]
        remote(ref, ref, b_send.at[0], sem.at[g], base + g).wait_recv()

    loads[10].wait()
    loads[11].wait()

    def copy_w(g):
        return remote(send_w.at[rows_of(g)], recv_w.at[me], w_send.at[g], w_recv.at[me], base + g)

    def copy_s(g):
        return remote(send_s.at[rows_of(g)], recv_s.at[me], s_send.at[g], s_recv.at[me], base + g)

    place = me * positions + lax.broadcasted_iota(jnp.int32, (1, positions), 1)

    def attend(t):
        g = near(t)

        @pl.when(base + g != me)
        def _():
            arrive(qbuf, b_recv, g)

        for j in range(owned):
            s = g * owned + j
            q = qbuf[pl.ds(s, 1)][0].astype(f32)
            both = jnp.concatenate(
                [jnp.where(low_map, q, 0.0), jnp.where(low_map, 0.0, q)], axis=0
            ).astype(bf16)
            scores = (
                lax.dot_general(
                    both,
                    ck[pl.ds(s, 1)][0],
                    (((1,), (1,)), ((), ())),
                    preferred_element_type=f32,
                )
                * scale
            )
            valid = place < lengths[s]
            highest = jnp.max(jnp.where(valid, scores, masked_score), axis=1, keepdims=True)
            expo = jnp.where(valid, jnp.exp(scores - highest), 0.0)
            summed = jnp.sum(expo, axis=1, keepdims=True)
            send_s[pl.ds(s, 1)] = jnp.concatenate([to_lanes(highest), to_lanes(summed)], axis=0)[
                None
            ]
            send_w[pl.ds(s, 1)] = jnp.dot(
                expo.astype(bf16), cv[pl.ds(s, 1)][0], preferred_element_type=f32
            ).astype(bf16)[None]

        @pl.when(base + g != me)
        def _():
            copy_s(g).start()
            copy_w(g).start()

    over(0, owners, attend)

    def arrive_k(g):
        @pl.when(base + g != me)
        def _():
            arrive(nbuf, k_recv, g)

    over(0, owners, arrive_k)
    entries = [nbuf[s].astype(f32) for s in range(rows)]
    nk_o[...] = jnp.concatenate([e[0:1] for e in entries], axis=0).astype(bf16)
    nv_o[...] = jnp.concatenate([e[1:2] for e in entries], axis=0).astype(bf16)

    def copy_e(peer, other):
        ref = att.at[core, rows_of(mine)]
        return remote(
            ref,
            ref,
            e_send.at[peer * n_tp + other],
            e_recv.at[mine * n_tp + core],
            peer,
            other,
        )

    def each_e(run):
        for other, c in cores():
            over(0 if c else 1, n_kv, lambda o: run(copy_e(peer_of(o), other)))

    @pl.when(is_owner)
    def _():
        recv_w[pl.ds(me, 1)] = send_w[rows_of(mine)][None]
        recv_s[pl.ds(me, 1)] = send_s[rows_of(mine)][None]
        weigh = jnp.where(lane < heads, 1.0, 0.0)
        for h in range(heads):
            weigh = jnp.where(lane == heads + h, -lambdas[h], weigh)
        owns = []
        for j in range(owned):
            query = qbuf[pl.ds(mine * owned + j, 1)][0].astype(f32)
            entry = nbuf[pl.ds(mine * owned + j, 1)][0].astype(f32)
            dots = query * entry[0:1]
            own_lo = jnp.sum(jnp.where(low_map, dots, 0.0), axis=1, keepdims=True)
            own_hi = jnp.sum(jnp.where(low_map, 0.0, dots), axis=1, keepdims=True)
            own = to_lanes(jnp.concatenate([own_lo, own_hi], axis=0) * scale)
            owns.append((own, entry[1:2]))

        def wait_s(o):
            peer = peer_of(o)
            remote(
                send_s.at[rows_of(0)], recv_s.at[peer], s_send.at[0], s_recv.at[peer], peer
            ).wait_recv()

        def wait_w(o):
            peer = peer_of(o)
            remote(
                send_w.at[rows_of(0)], recv_w.at[peer], w_send.at[0], w_recv.at[peer], peer
            ).wait_recv()

        over(1, n_kv, wait_s)
        shares = []
        for j in range(owned):
            own, new_value = owns[j]
            highest = gather(n_kv, lambda i, m: jnp.maximum(m, recv_s[i, j, 0:1, :]), own)
            own_weight = jnp.exp(own - highest)
            total = gather(
                n_kv,
                lambda i, t: t
                + recv_s[i, j, 1:2, :] * jnp.exp(recv_s[i, j, 0:1, :] - highest),
                own_weight,
            )
            share = weigh / total
            shares.append((highest, share, to_column(share * own_weight) * new_value))
        over(1, n_kv, wait_w)
        for j in range(owned):
            highest, share, start = shares[j]
            both = gather(
                n_kv,
                lambda i, t: t
                + recv_w[i, j].astype(f32)
                * to_column(share * jnp.exp(recv_s[i, j, 0:1, :] - highest)),
                start,
            )
            gaps = both[:heads] + both[heads:]
            mean = jnp.mean(gaps * gaps, axis=1, keepdims=True)
            normed = gaps * lax.rsqrt(mean + epsilon) * hg[...]
            att[core, pl.ds(mine * owned + j, 1)] = (normed * output_scale).astype(bf16)[None]
        each_e(lambda copy: copy.start())

    loads[12].wait()

    def project(other, c):
        def wait(g):
            def run():
                ref = att.at[other, rows_of(g)]
                remote(
                    ref, ref, e_send.at[0], e_recv.at[g * n_tp + other], base + g, other
                ).wait_recv()

            if c:
                run()
            else:
                pl.when(base + g != me)(run)

        over(0, owners, wait)
        att_f[...] = att[pl.ds(other, 1)][0].astype(f32).reshape(rows * heads, width)
        attended = jnp.concatenate(
            [att_f[pl.ds(h, rows, stride=heads), :] for h in range(heads)], axis=1
        ).astype(bf16)
        part = jnp.dot(attended, wo[pl.ds(other, 1)][0], preferred_element_type=f32)
        return part.astype(bf16).astype(f32)

    for other, c in cores():
        if c:
            remote(
                wo_h, wo.at[other], o_send.at[0], o_recv.at[other], me, other
            ).wait_recv()
    mixed = jnp.zeros(mixed_o.shape, f32)
    for other, c in cores():
        mixed = mixed + project(other, c)
    mixed_o[...] = mixed.astype(bf16)

    def sent(g):
        @pl.when(base + g != me)
        def _():
            copy_a(g).wait_send()
            copy_n(g).wait_send()
            copy_s(g).wait_send()
            copy_w(g).wait_send()

    over(0, owners, sent)

    @pl.when(is_owner)
    def _():
        def sent_all(o):
            copy_b(peer_of(o)).wait_send()
            copy_k(peer_of(o)).wait_send()

        over(1, n_kv, sent_all)
        each_e(lambda copy: copy.wait_send())

    for other, c in cores():
        if c:
            copy_o(other).wait_send()


def owner_plan(n_kv, rows):
    owners = max(1, min(n_kv // 2, rows))
    return owners, rows // owners, (n_kv - owners) // 2


def emit(*refs):
    count = (len(refs) - 1) // 2
    sem = refs[-1]
    copies = [
        pltpu.make_async_copy(refs[i], refs[count + i], sem.at[i]) for i in range(count)
    ]
    for copy in copies:
        copy.start()
    for copy in copies:
        copy.wait()


def body(
    n_kv,
    n_tp,
    tokens,
    lengths,
    query_weight,
    key_weight,
    value_weight,
    query_gain,
    key_gain,
    lambdas,
    head_gain,
    out_weight,
    cache_keys,
    cache_values,
):
    rows, positions, kv_heads, width = cache_keys.shape
    assert kv_heads == 1 and key_weight.shape[1] == width
    half = width // 2
    quarter = half // 2
    heads = query_weight.shape[1] // width
    owners, owned, _ = owner_plan(n_kv, rows)
    assert owners * owned == rows
    ck = cache_keys.reshape(rows, positions, width)
    cv = cache_values.reshape(rows, positions, width)
    exponent = -(np.arange(width) % quarter) / quarter
    freq = jnp.asarray((rotary_base**exponent).astype(np.float32)[None])
    qg = query_gain.reshape(1, half)
    kg = key_gain.reshape(1, half)
    hg = head_gain.reshape(1, width)
    held = [tokens, query_weight, key_weight, value_weight, freq, qg, kg, hg, ck, cv]
    dma = pltpu.SemaphoreType.DMA
    hbm = pl.BlockSpec(memory_space=pl.ANY)
    vmem = pl.BlockSpec(memory_space=pltpu.VMEM)
    out_columns = out_weight.shape[1]
    shapes = [(rows, out_columns), (rows, width), (rows, width)]
    results = pl.pallas_call(
        functools.partial(kernel, n_kv, n_tp),
        name="decode_step",
        out_shape=[pltpu.VMEM(shape, bf16) for shape in shapes],
        in_specs=[hbm] * (3 + len(held)),
        out_specs=[vmem] * 3,
        scratch_shapes=[
            pltpu.SMEM(lengths.shape, lengths.dtype),
            pltpu.SMEM(lambdas.shape, lambdas.dtype),
        ]
        + [pltpu.VMEM(a.shape, a.dtype) for a in held]
        + [
            pltpu.VMEM((n_tp, *out_weight.shape), bf16),
            pltpu.VMEM((rows, heads, width), f32),
            pltpu.VMEM((n_kv, owned, heads, width), f32),
            pltpu.VMEM((rows, 2, width), f32),
            pltpu.VMEM((n_kv, owned, 2, width), f32),
            pltpu.VMEM((rows, heads, width), bf16),
            pltpu.VMEM((rows, 2, width), bf16),
            pltpu.VMEM((rows, 2 * heads, width), bf16),
            pltpu.VMEM((rows, 2, width), f32),
            pltpu.VMEM((n_kv, owned, 2 * heads, width), bf16),
            pltpu.VMEM((n_kv, owned, 2, width), f32),
            pltpu.VMEM((n_tp, rows, heads, width), bf16),
            pltpu.VMEM((rows * heads, width), f32),
            dma((3 + len(held),)),
            dma((owners,)),
            dma((n_kv,)),
            dma((owners,)),
            dma((n_kv,)),
            dma((n_kv,)),
            dma((owners,)),
            dma((n_kv,)),
            dma((owners,)),
            dma((owners,)),
            dma((n_kv,)),
            dma((owners,)),
            dma((n_kv,)),
            dma((n_kv * n_tp,)),
            dma((owners * n_tp,)),
            dma((n_tp,)),
            dma((n_tp,)),
        ],
        compiler_params=pltpu.CompilerParams(collective_id=0, has_side_effects=True),
    )(lengths, lambdas, *held, out_weight)
    mixed, new_keys, new_values = pl.pallas_call(
        emit,
        name="emit",
        out_shape=[jax.ShapeDtypeStruct(shape, bf16) for shape in shapes],
        in_specs=[vmem] * 3,
        out_specs=[hbm] * 3,
        scratch_shapes=[dma((3,))],
    )(*[pltpu.with_memory_space_constraint(r, pltpu.VMEM) for r in results])
    return (
        mixed,
        new_keys.reshape(rows, kv_heads, width),
        new_values.reshape(rows, kv_heads, width),
    )


def solution(mesh):
    return jax.shard_map(
        functools.partial(body, mesh.shape["kv"], mesh.shape["tp"]),
        mesh=mesh,
        in_specs=(
            P("dp", "kv"),
            P("dp"),
            P("kv", "tp"),
            P("kv", "tp"),
            P("kv", "tp"),
            P(),
            P(),
            P("tp"),
            P(),
            P("tp", "kv"),
            P("dp", "kv", "tp", None),
            P("dp", "kv", "tp", None),
        ),
        out_specs=(P("dp", "kv"), P("dp", "tp", None), P("dp", "tp", None)),
        check_vma=False,
    )
```

time: 31.8 us -> 24.1 us (0.76)
  Pallas kernels: 28.3 us -> 23.3 us
  local copies, waits for them, and re-layouts: 2.59 us -> 0 us
    pallas_call x1, Pallas kernels: 28.3 us -> 22.7 us  [body(): pl.pallas_call(functools.partial(kernel, n_kv, n_tp), name='decode_step',...]
    unnamed x9 -> x0, local copies, waits for them, and re-layouts: 2.59 us -> none
    pallas_call x0 -> x1, Pallas kernels: none -> 0.63 us  [body(): pl.pallas_call(emit, name='emit', out_shape=[jax.ShapeDtypeStruct(shape,...]
where the time goes in v2:
time: 24.1 us; the launch traced here: 23.9 us
  Pallas kernels  23.3 us (97%)
  between operations  0.64 us (3%)
    pallas_call x1, Pallas kernels, body(): pl.pallas_call(functools.partial(kernel, n_kv, n_tp), name='decode_step',...  22.7 us
    pallas_call x1, Pallas kernels, body(): pl.pallas_call(emit, name='emit', out_shape=[jax.ShapeDtypeStruct(shape,...  0.63 us

profile of v2, /device:TPU:0, one launch (start us, length us, event | category | flops | bytes accessed | tf_op | source)
XLA Modules:
  0.0 23.9 jit_solution(572551720072851517)
XLA Ops:
  0.6 22.7 %decode_step.1 = (bf16[8,256]{1,0:T(8,128)(2,1)S(1)}, bf16[8,128]{1,0:T(8,128)(2,1)S(1)}, bf16[8,128]{1,0:T(8,128)(2,1)S(1)}) custom-call(s32[8]{0:T(128)} %lengths_h.1, f32[8]{0:T(128)} %lambdas_h.1, bf16[8,256]{1,0:T(8,128)(2,1)} %tokens_h.1, bf16[256,1024]{1,0:T(8,128)(2,1)} %wq_h.1, bf16[256,128]{1,0:T(8,128)(2,1)} %wk_h.1, bf16[256,128]{1,0:T(8,128)(2,1)} %wv_h.1, ...), custom_call_target="tpu_custom_call" | custom-call | tf_op jit(solution)/shard_map/decode_step/pallas_call | solution.py:545
  23.3 0.6 %emit.1 = (bf16[8,256]{1,0:T(8,128)(2,1)}, bf16[8,128]{1,0:T(8,128)(2,1)}, bf16[8,128]{1,0:T(8,128)(2,1)}) custom-call(bf16[8,256]{1,0:T(8,128)(2,1)S(1)} %get-tuple-element.9.refs_0_, bf16[8,128]{1,0:T(8,128)(2,1)S(1)} %get-tuple-element.10.refs_1_, bf16[8,128]{1,0:T(8,128)(2,1)S(1)} %get-tuple-element.11.refs_2_), custom_call_target="tpu_custom_call" | custom-call | tf_op jit(solution)/shard_map/emit/pallas_call | solution.py:590

commit v3 on v2

--- a/solution.py
+++ b/solution.py
@@ -84,6 +84,8 @@
     recv_s,
     att,
     att_f,
+    keys_t,
+    bias,
     load_sem,
     a_send,
     a_recv,
@@ -145,6 +147,10 @@
     def peer_of(o):
         return lax.rem(me + o, n_kv)
 
+    def far(o):
+        swing = (o // 2) * (2 * (o % 2) - 1)
+        return lax.rem(me + n_kv // 2 + swing + n_kv, n_kv)
+
     @pl.when(is_owner)
     def _():
         for other, c in cores():
@@ -200,7 +206,10 @@
 
     upper = (2 * me) // n_kv
 
+    swap = (me + upper) % 2 if owners % 2 == 0 else 0
+
     def near(t):
+        t = t + swap * (1 - 2 * (t % 2))
         return t + upper * (owners - 1 - 2 * t)
 
     def start_a(t):
@@ -209,9 +218,16 @@
         @pl.when(base + g != me)
         def _():
             copy_a(g).start()
+
+    def start_n(t):
+        g = near(owners - 1 - t)
+
+        @pl.when(base + g != me)
+        def _():
             copy_n(g).start()
 
     over(0, owners, start_a)
+    over(0, owners, start_n)
 
     def copy_o(other):
         return remote(wo_h, wo.at[core], o_send.at[other], o_recv.at[core], me, other)
@@ -235,6 +251,13 @@
 
     for load in loads[4:10]:
         load.wait()
+
+    loads[10].wait()
+    for s in range(rows):
+        keys_t[s] = ck[s].T
+    place = me * positions + lax.broadcasted_iota(jnp.int32, (1, positions), 1)
+    for s in range(rows):
+        bias[s] = jnp.where(place < lengths[s], 0.0, masked_score)
 
     def copy_b(peer):
         ref = qbuf.at[rows_of(mine)]
@@ -284,20 +307,19 @@
         for j in range(owned):
             total = gather(n_kv, lambda i, t: t + recv_a[i, j], jnp.zeros((heads, width), f32))
             qbuf[pl.ds(mine * owned + j, 1)] = turned(total, gain_q, turns[j]).astype(bf16)[None]
-        over(1, n_kv, lambda o: copy_b(peer_of(o)).start())
+        over(1, n_kv, lambda o: copy_b(far(o)).start())
         over(1, n_kv, wait_n)
         first = lax.broadcasted_iota(jnp.int32, (2, width), 0) == 0
         for j in range(owned):
             total = gather(n_kv, lambda i, t: t + recv_n[i, j], jnp.zeros((2, width), f32))
             entry = jnp.where(first, turned(total, gain_k, turns[j]), total)
             nbuf[pl.ds(mine * owned + j, 1)] = entry.astype(bf16)[None]
-        over(1, n_kv, lambda o: copy_k(peer_of(o)).start())
+        over(1, n_kv, lambda o: copy_k(far(o)).start())
 
     def arrive(buf, sem, g):
         ref = buf.at[rows_of(g)]
         remote(ref, ref, b_send.at[0], sem.at[g], base + g).wait_recv()
 
-    loads[10].wait()
     loads[11].wait()
 
     def copy_w(g):
@@ -305,8 +327,6 @@
 
     def copy_s(g):
         return remote(send_s.at[rows_of(g)], recv_s.at[me], s_send.at[g], s_recv.at[me], base + g)
-
-    place = me * positions + lax.broadcasted_iota(jnp.int32, (1, positions), 1)
 
     def attend(t):
         g = near(t)
@@ -321,18 +341,10 @@
             both = jnp.concatenate(
                 [jnp.where(low_map, q, 0.0), jnp.where(low_map, 0.0, q)], axis=0
             ).astype(bf16)
-            scores = (
-                lax.dot_general(
-                    both,
-                    ck[pl.ds(s, 1)][0],
-                    (((1,), (1,)), ((), ())),
-                    preferred_element_type=f32,
-                )
-                * scale
-            )
-            valid = place < lengths[s]
-            highest = jnp.max(jnp.where(valid, scores, masked_score), axis=1, keepdims=True)
-            expo = jnp.where(valid, jnp.exp(scores - highest), 0.0)
+            dots = jnp.dot(both, keys_t[pl.ds(s, 1)][0], preferred_element_type=f32)
+            scores = dots * scale + bias[pl.ds(s, 1)][0]
+            highest = jnp.max(scores, axis=1, keepdims=True)
+            expo = jnp.exp(scores - highest)
             summed = jnp.sum(expo, axis=1, keepdims=True)
             send_s[pl.ds(s, 1)] = jnp.concatenate([to_lanes(highest), to_lanes(summed)], axis=0)[
                 None
@@ -370,8 +382,14 @@
         )
 
     def each_e(run):
+        def each(o):
+            for other, _ in cores():
+                run(copy_e(far(o), other))
+
+        over(1, n_kv, each)
         for other, c in cores():
-            over(0 if c else 1, n_kv, lambda o: run(copy_e(peer_of(o), other)))
+            if c:
+                run(copy_e(me, other))
 
     @pl.when(is_owner)
     def _():
@@ -567,6 +585,8 @@
             pltpu.VMEM((n_kv, owned, 2, width), f32),
             pltpu.VMEM((n_tp, rows, heads, width), bf16),
             pltpu.VMEM((rows * heads, width), f32),
+            pltpu.VMEM((rows, width, positions), bf16),
+            pltpu.VMEM((rows, 1, positions), f32),
             dma((3 + len(held),)),
             dma((owners,)),
             dma((n_kv,)),

time: 24.1 us -> 23.3 us (0.967)
  Pallas kernels: 23.3 us -> 22.5 us
    pallas_call x1, Pallas kernels: 22.7 us -> 21.8 us  [body(): pl.pallas_call(functools.partial(kernel, n_kv, n_tp), name='decode_step',...]
where the time goes in v3:
time: 23.3 us; the launch traced here: 23.1 us
  Pallas kernels  22.5 us (97%)
  between operations  0.64 us (3%)
    pallas_call x1, Pallas kernels, body(): pl.pallas_call(functools.partial(kernel, n_kv, n_tp), name='decode_step',...  21.8 us
    pallas_call x1, Pallas kernels, body(): pl.pallas_call(emit, name='emit', out_shape=[jax.ShapeDtypeStruct(shape,...  0.63 us

profile of v3, /device:TPU:0, one launch (start us, length us, event | category | flops | bytes accessed | tf_op | source)
XLA Modules:
  0.0 23.1 jit_solution(9341118014998691138)
XLA Ops:
  0.6 21.8 %decode_step.1 = (bf16[8,256]{1,0:T(8,128)(2,1)S(1)}, bf16[8,128]{1,0:T(8,128)(2,1)S(1)}, bf16[8,128]{1,0:T(8,128)(2,1)S(1)}) custom-call(s32[8]{0:T(128)} %lengths_h.1, f32[8]{0:T(128)} %lambdas_h.1, bf16[8,256]{1,0:T(8,128)(2,1)} %tokens_h.1, bf16[256,1024]{1,0:T(8,128)(2,1)} %wq_h.1, bf16[256,128]{1,0:T(8,128)(2,1)} %wk_h.1, bf16[256,128]{1,0:T(8,128)(2,1)} %wv_h.1, ...), custom_call_target="tpu_custom_call" | custom-call | tf_op jit(solution)/shard_map/decode_step/pallas_call | solution.py:563
  22.5 0.6 %emit.1 = (bf16[8,256]{1,0:T(8,128)(2,1)}, bf16[8,128]{1,0:T(8,128)(2,1)}, bf16[8,128]{1,0:T(8,128)(2,1)}) custom-call(bf16[8,256]{1,0:T(8,128)(2,1)S(1)} %get-tuple-element.9.refs_0_, bf16[8,128]{1,0:T(8,128)(2,1)S(1)} %get-tuple-element.10.refs_1_, bf16[8,128]{1,0:T(8,128)(2,1)S(1)} %get-tuple-element.11.refs_2_), custom_call_target="tpu_custom_call" | custom-call | tf_op jit(solution)/shard_map/emit/pallas_call | solution.py:610
